TPU v7x, 32 devices: a whole 2x2x4 slice. The times are simulated.
32 devices in a mesh: sp: 8 (over z, x), dp: 4 (over y, core).
Axes of the slice: x: 2, y: 2, z: 4, core: 2. Of those that a mesh axis runs over, the one named last changes fastest.
Arguments:
- queries: bfloat16 [16, 8, 512, 256], P('dp', None, 'sp'), may hold values from -6 to 6
- keys: bfloat16 [16, 8, 512, 256], P('dp', None, 'sp'), may hold values from -6 to 6
- values: bfloat16 [16, 8, 512, 256], P('dp', None, 'sp'), may hold values from -6 to 6
- log_decay: float32 [128, 512], P(('dp', 'sp')), may hold values from -2 to 0, as said below
- w_out: bfloat16 [8, 256, 2048], P(None, None, 'dp'), may hold values from -0.125 to 0.125
Outputs:
- mixed_out: bfloat16 [16, 512, 2048], P('dp', 'sp')
Inputs may be any that keep to these rules, and one draw needn't show every extreme that they name: Every entry of log_decay is below zero.
All inputs are finite; a program needn't handle non-finite values.
Results may differ from a plain program's by a relative error of at most 0.008.
Values may be sent and summed in bfloat16 or wider, within the bound.
A program may use at most 128 MiB of HBM per device.

v0:
```python
import jax
import jax.numpy as jnp
from jax import lax
from jax.sharding import PartitionSpec as P

BLOCK = 64


def rotate(field_in, cosine, sine_tab):
    half_dim = field_in.shape[1] // 2
    widened = field_in.astype(jnp.float32)
    first_half = widened[:, :half_dim]
    second_half = widened[:, half_dim:]
    turned = jnp.concatenate(
        [
            first_half * cosine - second_half * sine_tab,
            second_half * cosine + first_half * sine_tab,
        ],
        axis=1,
    )
    return turned.astype(jnp.bfloat16)


def retain(query_rows, key_rows, value_rows, decay_row, cosine, sine_tab):
    length, head_width = query_rows.shape
    blocks = length // BLOCK
    rot_query = rotate(query_rows, cosine, sine_tab).reshape(blocks, BLOCK, head_width)
    rot_key = rotate(key_rows, cosine, sine_tab).reshape(blocks, BLOCK, head_width)
    value_blocks = value_rows.reshape(blocks, BLOCK, head_width)
    within = jnp.cumsum(decay_row.reshape(blocks, BLOCK), axis=1)
    ending = within[:, -1:]
    causal = jnp.tril(jnp.ones((BLOCK, BLOCK), dtype=bool))[None]
    spread = within[:, :, None] - within[:, None, :]
    decay_mask = jnp.where(causal, jnp.exp(jnp.where(causal, spread, 0.0)), 0.0)
    scores = jnp.einsum("bnd,bmd->bnm", rot_query, rot_key, preferred_element_type=jnp.float32)
    weights = (scores * decay_mask).astype(jnp.bfloat16)
    scaled_keys = (rot_key * jnp.exp(ending - within)[:, :, None]).astype(jnp.bfloat16)
    updates = jnp.einsum(
        "bmd,bme->bde", scaled_keys, value_blocks, preferred_element_type=jnp.float32
    )

    def advance(state_now, inputs):
        factor, update = inputs
        return (factor * state_now + update, state_now.astype(jnp.bfloat16))

    start_state = jnp.zeros((head_width, head_width), jnp.float32)
    _, before = lax.scan(advance, start_state, (jnp.exp(ending[:, 0]), updates))
    local_part = jnp.einsum(
        "bnm,bme->bne", weights, value_blocks, preferred_element_type=jnp.float32
    )
    carried = jnp.einsum("bnd,bde->bne", rot_query, before, preferred_element_type=jnp.float32)
    combined = local_part + jnp.exp(within)[:, :, None] * carried
    return combined.reshape(length, head_width).astype(jnp.bfloat16)


def on_device(queries, keys, values, log_decay, w_out):
    groups, head_count, seg_len, head_width = queries.shape
    item_count = groups * head_count
    flat_q = queries.reshape(item_count, seg_len, head_width)
    flat_k = keys.reshape(item_count, seg_len, head_width)
    flat_v = values.reshape(item_count, seg_len, head_width)
    head_k, head_v = (
        lax.all_to_all(flat_k, "sp", split_axis=0, concat_axis=1, tiled=True),
        lax.all_to_all(flat_v, "sp", split_axis=0, concat_axis=1, tiled=True),
    )
    head_q = lax.all_to_all(flat_q, "sp", split_axis=0, concat_axis=1, tiled=True)
    length = head_q.shape[1]
    half_dim = head_width // 2
    frequency = 10000.0 ** (-jnp.arange(half_dim, dtype=jnp.float32) / half_dim)
    angles = jnp.arange(length, dtype=jnp.float32)[:, None] * frequency[None, :]
    cosine = jnp.cos(angles)
    sine_tab = jnp.sin(angles)

    def one_item(inputs):
        return retain(inputs[0], inputs[1], inputs[2], inputs[3], cosine, sine_tab)

    retained = lax.map(one_item, (head_q, head_k, head_v, log_decay))
    by_token = lax.all_to_all(retained, "sp", split_axis=1, concat_axis=0, tiled=True)
    by_token = by_token.reshape(groups, head_count, seg_len, head_width)
    widened = by_token.astype(jnp.float32)
    normed = (
        widened * lax.rsqrt(jnp.mean(widened * widened, axis=-1, keepdims=True) + 1e-06)
    ).astype(jnp.bfloat16)
    mixed_out = jnp.einsum(
        "shtd,hde->ste",
        normed,
        lax.all_gather(w_out, "dp", axis=2, tiled=True),
        preferred_element_type=jnp.float32,
    )
    return mixed_out.astype(jnp.bfloat16)


def solution(mesh):
    placed = (
        P("dp", None, "sp", None),
        P("dp", None, "sp", None),
        P("dp", None, "sp", None),
        P(("dp", "sp"), None),
        P(None, None, "dp"),
    )
    return jax.shard_map(
        on_device, mesh=mesh, in_specs=placed, out_specs=P("dp", "sp", None), check_vma=False
    )
```

profile of v0, /device:TPU:0, one launch (start us, length us, event | category | flops | bytes accessed | tf_op | source)
XLA Modules:
  0.0 242.2 jit_solution(14307589264207442078)
XLA Ops:
  6.5 33.2 %all_to_all.63 = bf16[32,64,256]{2,1,0:T(8,128)(2,1)S(1)} all-to-all(bf16[32,64,256]{2,1,0:T(8,128)(2,1)} %bitcast.108), channel_id=1, replica_groups=mesh['sp'=8,'dp'=4] {'sp'}, dimensions={0} | all-to-all | bytes 2097152 | tf_op jit(solution)/shard_map/all_to_all | solution.py:64
  39.7 28.8 %all_to_all.64 = bf16[32,64,256]{2,1,0:T(8,128)(2,1)S(1)} all-to-all(bf16[32,64,256]{2,1,0:T(8,128)(2,1)S(1)} %bitcast.109), channel_id=1, replica_groups=mesh['sp'=8,'dp'=4] {'sp'}, dimensions={0} | all-to-all | bytes 2097152 | tf_op jit(solution)/shard_map/all_to_all | solution.py:66
  68.6 3.6 %all-to-all-start.1 = ((bf16[32,64,256]{2,1,0:T(8,128)(2,1)}), bf16[32,64,256]{2,1,0:T(8,128)(2,1)S(1)}, u32[]{:S(2)}, u32[]{:S(2)}) async-start(bf16[32,64,256]{2,1,0:T(8,128)(2,1)} %bitcast.110), calls=%async_computation.1 | async-start | bytes 2097152 | tf_op jit(solution)/shard_map/all_to_all | solution.py:63
  72.9 1.0 copy.28
  73.9 1.1 copy.26
  75.1 22.6 %all-to-all-done.1 = bf16[32,64,256]{2,1,0:T(8,128)(2,1)S(1)} async-done(((bf16[32,64,256]{2,1,0:T(8,128)(2,1)}), bf16[32,64,256]{2,1,0:T(8,128)(2,1)S(1)}, u32[]{:S(2)}, u32[]{:S(2)}) %all-to-all-start.1) | async-done | bytes 1048608 | tf_op jit(solution)/shard_map/all_to_all | solution.py:63
  97.6 1.0 copy.27
  98.7 97.2 %while.30 = (s32[]{:T(128)}, bf16[4,512,256]{2,1,0:T(8,128)(2,1)}, bf16[4,512,256]{2,1,0:T(8,128)(2,1)}, bf16[4,512,256]{2,1,0:T(8,128)(2,1)}, f32[4,512]{1,0:T(...) while((s32[]{:T(128)}, bf16[4,512,256]{2,1,0:T(8,128)(2,1)}, ...), condition=%wide.region_4.5_spmd.clone.clone.clone, body=%wide.region_0.4_spmd.clone.clone.clone.sunk | while | flops 172363776 | bytes 15632365 | solution.py:77
  98.7 1.1 bitcast_convert_fusion.3
  99.8 1.2 fusion.70
  102.2 1.0 constant_dynamic-slice_fusion.2
  104.0 16.7 %while.31 = (s32[]{:T(128)}, f32[256,256]{1,0:T(8,128)S(1)}, bf16[8,256,256]{2,1,0:T(8,128)(2,1)}, f32[8]{0:T(128)S(1)}, f32[8,256,256]{2,1,0:T(8,128)S(1)}, /*index=5*/s32[]{:T(128)}, s32[]{:T(128)}) while((s32[]{:T(128)}, f32[256,256]{1,0:T(8,128)S(1)}, bf16[8,256,256]{2,1,0:T(8,128)(2,1)}, f32[8]{0:T(128)S(1)}, ...), condition=%wide.region_3.3_spmd.clone, body=%wide.region_2.2_spmd.clone.sunk | while | flops 262147 | bytes 1180268 | solution.py:47
  123.0 1.1 bitcast_convert_fusion.3
  124.1 1.2 fusion.70
  128.3 16.7 %while.31 = (s32[]{:T(128)}, f32[256,256]{1,0:T(8,128)S(1)}, bf16[8,256,256]{2,1,0:T(8,128)(2,1)}, f32[8]{0:T(128)S(1)}, f32[8,256,256]{2,1,0:T(8,128)S(1)}, /*index=5*/s32[]{:T(128)}, s32[]{:T(128)}) while((s32[]{:T(128)}, f32[256,256]{1,0:T(8,128)S(1)}, bf16[8,256,256]{2,1,0:T(8,128)(2,1)}, f32[8]{0:T(128)S(1)}, ...), condition=%wide.region_3.3_spmd.clone, body=%wide.region_2.2_spmd.clone.sunk | while | flops 262147 | bytes 1180268 | solution.py:47
  147.3 1.1 bitcast_convert_fusion.3
  148.4 1.2 fusion.70
  152.6 16.7 %while.31 = (s32[]{:T(128)}, f32[256,256]{1,0:T(8,128)S(1)}, bf16[8,256,256]{2,1,0:T(8,128)(2,1)}, f32[8]{0:T(128)S(1)}, f32[8,256,256]{2,1,0:T(8,128)S(1)}, /*index=5*/s32[]{:T(128)}, s32[]{:T(128)}) while((s32[]{:T(128)}, f32[256,256]{1,0:T(8,128)S(1)}, bf16[8,256,256]{2,1,0:T(8,128)(2,1)}, f32[8]{0:T(128)S(1)}, ...), condition=%wide.region_3.3_spmd.clone, body=%wide.region_2.2_spmd.clone.sunk | while | flops 262147 | bytes 1180268 | solution.py:47
  171.6 1.1 bitcast_convert_fusion.3
  172.7 1.2 fusion.70
  176.9 16.7 %while.31 = (s32[]{:T(128)}, f32[256,256]{1,0:T(8,128)S(1)}, bf16[8,256,256]{2,1,0:T(8,128)(2,1)}, f32[8]{0:T(128)S(1)}, f32[8,256,256]{2,1,0:T(8,128)S(1)}, /*index=5*/s32[]{:T(128)}, s32[]{:T(128)}) while((s32[]{:T(128)}, f32[256,256]{1,0:T(8,128)S(1)}, bf16[8,256,256]{2,1,0:T(8,128)(2,1)}, f32[8]{0:T(128)S(1)}, ...), condition=%wide.region_3.3_spmd.clone, body=%wide.region_2.2_spmd.clone.sunk | while | flops 262147 | bytes 1180268 | solution.py:47
  195.9 2.0 copy.29
  198.0 29.1 %all_to_all.65 = bf16[4,512,256]{2,0,1:T(4,128)(2,1)S(1)} all-to-all(bf16[4,512,256]{2,0,1:T(4,128)(2,1)S(1)} %copy.29), channel_id=1, replica_groups=mesh['sp'=8,'dp'=4] {'sp'}, dimensions={1} | all-to-all | bytes 2097152 | tf_op jit(solution)/shard_map/all_to_all | solution.py:78
  228.5 6.8 %fusion.48 = bf16[4,64,2048]{2,1,0:T(8,128)(2,1)} fusion(bf16[8,256,2048]{2,1,0:T(8,128)(2,1)} %all-gather.2.cloned.1.call-done, f32[4,8,64]{2,1,0:T(8,128)S(1)} %bitcast.112, f32[4,8,64,256]{3,2,1,0:T(8,128)S(1)} %bitcast.107), kind=kOutput, calls=%fused_computation.59 | convolution fusion | flops 2149056512 | bytes 11542528 | tf_op jit(solution)/shard_map/shtd,hde->ste/dot_general | solution.py:84
  (171 shorter events, 88.4 us)
Async XLA Ops:
  6.5 33.2 %copy-start.1 = (bf16[4,8,64,256]{3,2,1,0:T(8,128)(2,1)S(1)}, bf16[4,8,64,256]{3,2,1,0:T(8,128)(2,1)}, u32[]{:S(2)}) copy-start(bf16[4,8,64,256]{3,2,1,0:T(8,128)(2,1)} %param.9) | copy-start | bytes 3145732
  68.6 29.1 %all-to-all-start.1 = ((bf16[32,64,256]{2,1,0:T(8,128)(2,1)}), bf16[32,64,256]{2,1,0:T(8,128)(2,1)S(1)}, u32[]{:S(2)}, u32[]{:S(2)}) async-start(bf16[32,64,256]{2,1,0:T(8,128)(2,1)} %bitcast.110), calls=%async_computation.1 | async-start | bytes 2097152 | tf_op jit(solution)/shard_map/all_to_all | solution.py:63
  72.1 156.4 %all-gather.2.cloned.1.call-start = ((), (), s32[]{:S(2)}) async-start(), calls=%async_computation.4 | async-start | bytes 10485760 | tf_op jit(solution)/shard_map/all_gather | solution.py:87
  120.7 1.2 copy-start
  145.0 1.2 copy-start
  169.3 1.2 copy-start
  193.7 1.2 copy-start
Sparse Core Ops, SparseCore 0:
  74.5 59.6 all-gather.1
where the time goes:
time: 243 us; the launch traced here: 242 us
  blocking collectives  91.1 us (37%)
  other arithmetic  56.7 us (23%)
  local copies, waits for them, and re-layouts  40.7 us (17%)
  waiting for transfers between devices  23.3 us (10%)
  between operations  13.5 us (6%)
  matrix products  12.3 us (5%)
  starting transfers between devices  3.6 us (1%)
    all_to_all x1, blocking collectives, on_device(): lax.all_to_all(flat_v, 'sp', split_axis=0, concat_axis=1, tiled=True)  33.2 us
    all_to_all x1, blocking collectives, on_device(): lax.all_to_all(retained, 'sp', split_axis=1, concat_axis=0, tiled=True)  29.1 us
    all_to_all x1, blocking collectives, on_device(): lax.all_to_all(flat_q, 'sp', split_axis=0, concat_axis=1, tiled=True)  28.8 us
    add x32, other arithmetic, advance(): return (factor * state_now + update, state_now.astype(jnp.bfloat16))  24 us
    all_to_all x1, waiting for transfers between devices, on_device(): lax.all_to_all(flat_k, 'sp', split_axis=0, concat_axis=1, tiled=True)  22.6 us
    dynamic_update_slice x32, other arithmetic, retain(): _, before = lax.scan(advance, start_state, (jnp.exp(ending[:, 0]), updates))  21.5 us
    dynamic_slice x32, local copies, waits for them, and re-layouts, retain(): _, before = lax.scan(advance, start_state, (jnp.exp(ending[:, 0]), updates))  20.7 us
    dynamic_slice x8, local copies, waits for them, and re-layouts, on_device(): retained = lax.map(one_item, (head_q, head_k, head_v, log_decay))  6.8 us
  transfers between devices with their start and end apart: 2, of which 1 were waited for; matrix products, arithmetic and copies ran while one was open for 41% of the time, Pallas kernels for 0%

commit v1 on v0

v1 whole, which is shorter than its diff:
```python
import functools

import jax
import jax.numpy as jnp
from jax import lax
from jax.experimental import pallas as pl
from jax.experimental.pallas import tpu as pltpu
from jax.sharding import PartitionSpec as P

MESH = pl.DeviceIdType.MESH
F32 = jnp.float32
BF16 = jnp.bfloat16


def kernel(sizes, freq_ref, q_hbm, k_hbm, v_hbm, ld_hbm, w_hbm, out_ref,
           qbuf, kbuf, vbuf, ldbuf, ldrows, cos_tab, sin_tab, wbuf, tin, tout, obuf, xbuf,
           local_sem, ld_send, ld_recv, x_send, x_recv, t_send, t_recv, o_send, o_recv,
           wa_send, wa_recv, wb_send, wb_recv):
    sp, dp, group, cores = sizes
    seqs, heads, seg, width = q_hbm.shape
    stages = sp // group
    own = heads // group
    items = seqs * own
    span = group * seg
    half = width // 2
    rows = ld_hbm.shape[0]
    pairs = dp // cores
    feats = w_hbm.shape[1]

    me = lax.axis_index("sp")
    col = lax.axis_index("dp")
    z, x = lax.div(me, group), lax.rem(me, group)
    pair, core = lax.div(col, cores), lax.rem(col, cores)
    sibling = pair * cores + (cores - 1 - core)
    mine = pl.ds(pl.multiple_of(x * seg, seg), seg)

    barrier = pltpu.get_barrier_semaphore()
    for r in range(1, sp):
        pl.semaphore_signal(barrier, inc=1, device_id={"sp": lax.rem(me + r, sp)}, device_id_type=MESH)
    for r in range(1, pairs):
        pl.semaphore_signal(barrier, inc=1, device_id={"dp": lax.rem(col + cores * r, dp)}, device_id_type=MESH)
    if cores == 2:
        pl.semaphore_signal(barrier, inc=1, device_id={"dp": sibling}, device_id_type=MESH)

    local = [
        pltpu.make_async_copy(ld_hbm, ldbuf.at[me], local_sem.at[0]),
        pltpu.make_async_copy(k_hbm.at[:, pl.ds(x * own, own)], kbuf.at[:, :, mine], local_sem.at[1]),
        pltpu.make_async_copy(v_hbm.at[:, pl.ds(x * own, own)], vbuf.at[:, :, mine], local_sem.at[2]),
        pltpu.make_async_copy(q_hbm.at[:, pl.ds(x * own, own)], qbuf.at[:, :, mine], local_sem.at[3]),
        pltpu.make_async_copy(w_hbm, wbuf.at[col], local_sem.at[4]),
    ]
    for copy in local:
        copy.start()

    def ld_copy(r):
        return pltpu.make_async_remote_copy(
            src_ref=ld_hbm, dst_ref=ldbuf.at[me], send_sem=ld_send.at[r - 1], recv_sem=ld_recv.at[r - 1],
            device_id={"sp": lax.rem(me + r, sp)}, device_id_type=MESH)

    def x_copies(i, r):
        s, hh = lax.div(i, own), lax.rem(i, own)
        to = lax.rem(x + r, group)
        return [
            pltpu.make_async_remote_copy(
                src_ref=src.at[s, to * own + hh], dst_ref=dst.at[s, hh, mine],
                send_sem=x_send.at[n, r - 1, i], recv_sem=x_recv.at[n, r - 1, i],
                device_id={"sp": z * group + to}, device_id_type=MESH)
            for n, (src, dst) in enumerate(((k_hbm, kbuf), (v_hbm, vbuf), (q_hbm, qbuf)))
        ]

    def t_copy(i):
        return pltpu.make_async_remote_copy(
            src_ref=tout.at[i], dst_ref=tin.at[i], send_sem=t_send.at[i], recv_sem=t_recv.at[i],
            device_id={"sp": lax.rem(me + group, sp)}, device_id_type=MESH)

    def o_copy(i, r):
        s, hh = lax.div(i, own), lax.rem(i, own)
        to = lax.rem(x + r, group)
        return pltpu.make_async_remote_copy(
            src_ref=obuf.at[s, hh, pl.ds(pl.multiple_of(to * seg, seg), seg)],
            dst_ref=xbuf.at[pl.ds(pl.multiple_of(s * seg, seg), seg),
                            pl.ds(pl.multiple_of((x * own + hh) * width, width), width)],
            send_sem=o_send.at[r - 1, i], recv_sem=o_recv.at[r - 1, i],
            device_id={"sp": z * group + to}, device_id_type=MESH)

    def wa_copy(r):
        return pltpu.make_async_remote_copy(
            src_ref=w_hbm, dst_ref=wbuf.at[col], send_sem=wa_send.at[r - 1], recv_sem=wa_recv.at[r - 1],
            device_id={"dp": lax.rem(col + cores * r, dp)}, device_id_type=MESH)

    def wb_copy(r):
        shard = lax.rem(pair + pairs - r, pairs) * cores + core
        return pltpu.make_async_remote_copy(
            src_ref=w_hbm if r == 0 else wbuf.at[shard], dst_ref=wbuf.at[shard],
            send_sem=wb_send.at[r], recv_sem=wb_recv.at[r],
            device_id={"dp": sibling}, device_id_type=MESH)

    pl.semaphore_wait(barrier, (sp - 1) + (pairs - 1) + (cores - 1))

    for r in range(1, sp):
        ld_copy(r).start()

    @pl.loop(0, items)
    def _(i):
        for r in range(1, group):
            for copy in x_copies(i, r):
                copy.start()

    for r in range(1, pairs):
        wa_copy(r).start()
    if cores == 2:
        wb_copy(0).start()

    place = lax.broadcasted_iota(jnp.int32, (span, half), 0) + z * span
    angle = place.astype(F32) * freq_ref[...]
    cos_tab[...] = jnp.cos(angle)
    sin_tab[...] = jnp.sin(angle)

    @pl.when(z == 0)
    def _():
        tin[...] = jnp.zeros_like(tin)

    for copy in local[:4]:
        copy.wait()
    for r in range(1, sp):
        ld_copy(r).wait_recv()
    for n in range(sp):
        ldrows[pl.ds(n * rows, rows), :] = ldbuf[n, :, pl.ds(pl.multiple_of(z * span, span), span)]

    def rotate(field):
        wide = field.astype(F32)
        first, second = wide[:, :half], wide[:, half:]
        cosine, sine = cos_tab[...], sin_tab[...]
        return jnp.concatenate(
            [first * cosine - second * sine, second * cosine + first * sine], axis=1).astype(BF16)

    @pl.loop(0, items)
    def _(i):
        s, hh = lax.div(i, own), lax.rem(i, own)
        for r in range(1, group):
            for copy in x_copies(i, r):
                copy.wait_recv()
        rank = lax.broadcasted_iota(jnp.int32, (span, span), 0)
        lane = lax.broadcasted_iota(jnp.int32, (span, span), 1)
        causal = rank >= lane
        decay = ldrows[pl.ds(s * heads + x * own + hh, 1), :]
        within = jnp.sum(jnp.where(causal, decay, 0.0), axis=1, keepdims=True)
        across = jnp.sum(jnp.where(rank == lane, within, 0.0), axis=0, keepdims=True)
        ending = jnp.sum(decay, axis=1, keepdims=True)
        mask = jnp.where(causal, jnp.exp(jnp.where(causal, within - across, 0.0)), 0.0)
        rot_q = rotate(qbuf[s, hh])
        rot_k = rotate(kbuf[s, hh])
        value = vbuf[s, hh]
        scaled = (rot_k.astype(F32) * jnp.exp(jnp.minimum(ending - within, 0.0))).astype(BF16)
        update = lax.dot_general(scaled, value, (((0,), (0,)), ((), ())), preferred_element_type=F32)
        scores = lax.dot_general(rot_q, rot_k, (((1,), (1,)), ((), ())), preferred_element_type=F32)
        weights = (scores * mask).astype(BF16)
        here = jnp.dot(weights, value, preferred_element_type=F32)

        @pl.when(z > 0)
        def _():
            t_copy(i).wait_recv()

        before = tin[i]
        tout[i] = (jnp.exp(ending) * before.astype(F32) + update).astype(BF16)

        @pl.when(z < stages - 1)
        def _():
            t_copy(i).start()

        carried = jnp.dot(rot_q, before, preferred_element_type=F32)
        retained = (here + jnp.exp(within) * carried).astype(BF16).astype(F32)
        square = jnp.mean(retained * retained, axis=1, keepdims=True)
        obuf[s, hh] = (retained * lax.rsqrt(square + 1e-06)).astype(BF16)
        for r in range(1, group):
            o_copy(i, r).start()
        xbuf[pl.ds(pl.multiple_of(s * seg, seg), seg),
             pl.ds(pl.multiple_of((x * own + hh) * width, width), width)] = obuf[s, hh, mine]

    for r in range(1, pairs):
        wa_copy(r).wait_recv()
        if cores == 2:
            wb_copy(r).start()
    local[4].wait()
    if cores == 2:
        for r in range(pairs):
            wb_copy(r).wait_recv()

    @pl.loop(0, items)
    def _(i):
        for r in range(1, group):
            o_copy(i, r).wait_recv()

    @pl.loop(0, dp)
    def _(n):
        out_ref[:, pl.ds(pl.multiple_of(n * feats, feats), feats)] = jnp.dot(
            xbuf[...], wbuf[n], preferred_element_type=F32).astype(BF16)

    for r in range(1, sp):
        ld_copy(r).wait_send()
    for r in range(1, pairs):
        wa_copy(r).wait_send()
    if cores == 2:
        for r in range(pairs):
            wb_copy(r).wait_send()

    @pl.loop(0, items)
    def _(i):
        for r in range(1, group):
            for copy in x_copies(i, r):
                copy.wait_send()
            o_copy(i, r).wait_send()

        @pl.when(z < stages - 1)
        def _():
            t_copy(i).wait_send()


def on_device(sp, dp, queries, keys, values, log_decay, w_out):
    seqs, heads, seg, width = queries.shape
    rows, length = log_decay.shape
    group = 2 if sp % 2 == 0 and heads % 2 == 0 else 1
    cores = 2 if dp % 2 == 0 else 1
    pairs, own = dp // cores, heads // group
    items, span, half = seqs * own, group * seg, width // 2
    feats = w_out.shape[2]
    frequency = (10000.0 ** (-jnp.arange(half, dtype=F32) / half))[None, :]
    dma = pltpu.SemaphoreType.DMA
    some = lambda count: max(count, 1)
    hbm = pl.BlockSpec(memory_space=pl.ANY)
    vmem = pl.BlockSpec(memory_space=pltpu.VMEM)
    mixed = pl.pallas_call(
        functools.partial(kernel, (sp, dp, group, cores)),
        out_shape=jax.ShapeDtypeStruct((seqs * seg, dp * feats), BF16),
        in_specs=[vmem, hbm, hbm, hbm, hbm, hbm],
        out_specs=vmem,
        scratch_shapes=[
            pltpu.VMEM((seqs, own, span, width), BF16),
            pltpu.VMEM((seqs, own, span, width), BF16),
            pltpu.VMEM((seqs, own, span, width), BF16),
            pltpu.VMEM((sp, rows, length), F32),
            pltpu.VMEM((sp * rows, span), F32),
            pltpu.VMEM((span, half), F32),
            pltpu.VMEM((span, half), F32),
            pltpu.VMEM((dp, heads * width, feats), BF16),
            pltpu.VMEM((items, width, width), BF16),
            pltpu.VMEM((items, width, width), BF16),
            pltpu.VMEM((seqs, own, span, width), BF16),
            pltpu.VMEM((seqs * seg, heads * width), BF16),
            dma((5,)),
            dma((some(sp - 1),)), dma((some(sp - 1),)),
            dma((3, some(group - 1), items)), dma((3, some(group - 1), items)),
            dma((items,)), dma((items,)),
            dma((some(group - 1), items)), dma((some(group - 1), items)),
            dma((some(pairs - 1),)), dma((some(pairs - 1),)),
            dma((pairs,)), dma((pairs,)),
        ],
        compiler_params=pltpu.CompilerParams(
            collective_id=0, has_side_effects=True, vmem_limit_bytes=48 * 2**20),
    )(frequency, queries, keys, values, log_decay, w_out.reshape(heads * width, feats))
    return mixed.reshape(seqs, seg, dp * feats)


def solution(mesh):
    placed = (
        P("dp", None, "sp", None),
        P("dp", None, "sp", None),
        P("dp", None, "sp", None),
        P(("dp", "sp"), None),
        P(None, None, "dp"),
    )
    body = functools.partial(on_device, mesh.shape["sp"], mesh.shape["dp"])
    return jax.shard_map(
        body, mesh=mesh, in_specs=placed, out_specs=P("dp", "sp", None), check_vma=False
    )
```

time: 243 us -> 77.8 us (0.32)
  the two profiles are of different devices: /device:TPU:0 before, /device:TPU:29 now
where the time goes in v1:
time: 77.8 us; the launch traced here: 77.6 us
  Pallas kernels  72.2 us (93%)
  local copies, waits for them, and re-layouts  5.34 us (7%)
    pallas_call x1, Pallas kernels, on_device(): pl.pallas_call(functools.partial(kernel, (sp, dp, group, cores)), out_sha...  72.2 us
    unnamed x9, local copies, waits for them, and re-layouts  5.34 us

profile of v1, /device:TPU:29, one launch (start us, length us, event | category | flops | bytes accessed | tf_op | source)
XLA Modules:
  0.0 77.6 jit_solution(2706689538564302164)
XLA Ops:
  0.0 0.0 copy-start
  0.0 1.2 %copy-done = bf16[4,8,64,256]{3,2,1,0:T(8,128)(2,1)S(1)} copy-done((bf16[4,8,64,256]{3,2,1,0:T(8,128)(2,1)S(1)}, bf16[4,8,64,256]{3,2,1,0:T(8,128)(2,1)}, u32[]{:S(2)}) %copy-start) | copy-done | bytes 1048600
  1.2 0.0 copy-start.1
  1.2 1.2 %copy-done.1 = bf16[4,8,64,256]{3,2,1,0:T(8,128)(2,1)S(1)} copy-done((bf16[4,8,64,256]{3,2,1,0:T(8,128)(2,1)S(1)}, bf16[4,8,64,256]{3,2,1,0:T(8,128)(2,1)}, u32[]{:S(2)}) %copy-start.1) | copy-done | bytes 1048600
  2.5 0.0 copy-start.2
  2.5 1.2 %copy-done.2 = bf16[4,8,64,256]{3,2,1,0:T(8,128)(2,1)S(1)} copy-done((bf16[4,8,64,256]{3,2,1,0:T(8,128)(2,1)S(1)}, bf16[4,8,64,256]{3,2,1,0:T(8,128)(2,1)}, u32[]{:S(2)}) %copy-start.2) | copy-done | bytes 1048600
  3.7 0.0 copy-start.3
  3.7 0.7 copy-done.3
  4.4 72.2 %shard_map.55 = bf16[256,2048]{1,0:T(8,128)(2,1)S(1)} custom-call(f32[1,128]{1,0:T(1,128)S(1)} %multiply_power_fusion.freq_ref, bf16[4,8,64,256]{3,2,1,0:T(8,128)(2,1)S(1)} %copy-done, bf16[4,8,64,256]{3,2,1,0:T(8,128)(2,1)S(1)} %copy-done.1, bf16[4,8,64,256]{3,2,1,0:T(8,128)(2,1)S(1)} %copy-done.2, f32[4,512]{1,0:T(4,128)S(1)} %copy-done.3, ...), custom_call_target="tpu_custom_call" | custom-call | tf_op jit(solution)/shard_map/pallas_call | solution.py:232
  76.6 1.0 %copy.7 = bf16[4,64,2048]{2,1,0:T(8,128)(2,1)} copy(bf16[4,64,2048]{2,1,0:T(8,128)(2,1)S(1)} %bitcast.2) | data formatting | bytes 2097152
  (1 shorter events, 0.0 us)
Async XLA Ops:
  0.0 1.2 %copy-start = (bf16[4,8,64,256]{3,2,1,0:T(8,128)(2,1)S(1)}, bf16[4,8,64,256]{3,2,1,0:T(8,128)(2,1)}, u32[]{:S(2)}) copy-start(bf16[4,8,64,256]{3,2,1,0:T(8,128)(2,1)} %q_hbm.1) | copy-start | bytes 3145732
  1.2 1.2 %copy-start.1 = (bf16[4,8,64,256]{3,2,1,0:T(8,128)(2,1)S(1)}, bf16[4,8,64,256]{3,2,1,0:T(8,128)(2,1)}, u32[]{:S(2)}) copy-start(bf16[4,8,64,256]{3,2,1,0:T(8,128)(2,1)} %k_hbm.1) | copy-start | bytes 3145732
  2.5 1.2 %copy-start.2 = (bf16[4,8,64,256]{3,2,1,0:T(8,128)(2,1)S(1)}, bf16[4,8,64,256]{3,2,1,0:T(8,128)(2,1)}, u32[]{:S(2)}) copy-start(bf16[4,8,64,256]{3,2,1,0:T(8,128)(2,1)} %v_hbm.1) | copy-start | bytes 3145732
  3.7 0.7 copy-start.3

commit v2 on v1

v2 whole, which is shorter than its diff:
```python
import functools
import math

import jax
import jax.numpy as jnp
from jax import lax
from jax.experimental import pallas as pl
from jax.experimental.pallas import tpu as pltpu
from jax.sharding import PartitionSpec as P

MESH = pl.DeviceIdType.MESH
F32 = jnp.float32
BF16 = jnp.bfloat16


def kernel(sizes, q_hbm, k_hbm, v_hbm, ld_hbm, w_hbm, out_ref,
           qbuf, kbuf, vbuf, ldbuf, ldrows, cos_tab, sin_tab, wbuf, tin, tout, obuf, xbuf,
           ubuf, fall, rkbuf, most,
           local_sem, ld_send, ld_recv, x_send, x_recv, t_send, t_recv, o_send, o_recv,
           wa_send, wa_recv, wb_send, wb_recv):
    sp, dp, group, cores = sizes
    seqs, heads, seg, width = q_hbm.shape
    stages = sp // group
    own = heads // group
    items = seqs * own
    span = group * seg
    half = width // 2
    rows = ld_hbm.shape[0]
    pairs = dp // cores
    feats = w_hbm.shape[1]
    parts = t_send.shape[1]
    slab = width // parts
    cuts = wa_send.shape[1]
    deep = heads * width // cuts

    me = lax.axis_index("sp")
    col = lax.axis_index("dp")
    z, x = lax.div(me, group), lax.rem(me, group)
    pair, core = lax.div(col, cores), lax.rem(col, cores)
    sibling = pair * cores + (cores - 1 - core)
    mine = pl.ds(pl.multiple_of(x * seg, seg), seg)

    barrier = pltpu.get_barrier_semaphore()
    for r in range(1, sp):
        pl.semaphore_signal(barrier, inc=1, device_id={"sp": lax.rem(me + r, sp)}, device_id_type=MESH)
    for r in range(1, pairs):
        pl.semaphore_signal(barrier, inc=1, device_id={"dp": lax.rem(col + cores * r, dp)}, device_id_type=MESH)
    if cores == 2:
        pl.semaphore_signal(barrier, inc=1, device_id={"dp": sibling}, device_id_type=MESH)

    local = [
        pltpu.make_async_copy(ld_hbm, ldbuf.at[me], local_sem.at[0]),
        pltpu.make_async_copy(k_hbm.at[:, pl.ds(x * own, own)], kbuf.at[:, :, mine], local_sem.at[1]),
        pltpu.make_async_copy(v_hbm.at[:, pl.ds(x * own, own)], vbuf.at[:, :, mine], local_sem.at[2]),
        pltpu.make_async_copy(q_hbm.at[:, pl.ds(x * own, own)], qbuf.at[:, :, mine], local_sem.at[3]),
        pltpu.make_async_copy(w_hbm, wbuf.at[col], local_sem.at[4]),
    ]
    for copy in local:
        copy.start()

    def ld_copy(r):
        return pltpu.make_async_remote_copy(
            src_ref=ld_hbm, dst_ref=ldbuf.at[me], send_sem=ld_send.at[r - 1], recv_sem=ld_recv.at[r - 1],
            device_id={"sp": lax.rem(me + r, sp)}, device_id_type=MESH)

    def x_copy(i, r, n):
        s, hh = lax.div(i, own), lax.rem(i, own)
        to = lax.rem(x + r, group)
        src, dst = ((k_hbm, kbuf), (v_hbm, vbuf), (q_hbm, qbuf))[n]
        return pltpu.make_async_remote_copy(
            src_ref=src.at[s, to * own + hh], dst_ref=dst.at[s, hh, mine],
            send_sem=x_send.at[n, r - 1, i], recv_sem=x_recv.at[n, r - 1, i],
            device_id={"sp": z * group + to}, device_id_type=MESH)

    def t_copy(i, p):
        some = pl.ds(p * slab, slab)
        return pltpu.make_async_remote_copy(
            src_ref=tout.at[i, some], dst_ref=tin.at[i, some], send_sem=t_send.at[i, p], recv_sem=t_recv.at[i, p],
            device_id={"sp": lax.rem(me + group, sp)}, device_id_type=MESH)

    def o_copy(i, r):
        s, hh = lax.div(i, own), lax.rem(i, own)
        to = lax.rem(x + r, group)
        return pltpu.make_async_remote_copy(
            src_ref=obuf.at[s, hh, pl.ds(pl.multiple_of(to * seg, seg), seg)],
            dst_ref=xbuf.at[pl.ds(pl.multiple_of(s * seg, seg), seg),
                            pl.ds(pl.multiple_of((x * own + hh) * width, width), width)],
            send_sem=o_send.at[r - 1, i], recv_sem=o_recv.at[r - 1, i],
            device_id={"sp": z * group + to}, device_id_type=MESH)

    def wa_copy(r, c):
        some = pl.ds(c * deep, deep)
        return pltpu.make_async_remote_copy(
            src_ref=w_hbm.at[some], dst_ref=wbuf.at[col, some],
            send_sem=wa_send.at[r - 1, c], recv_sem=wa_recv.at[r - 1, c],
            device_id={"dp": lax.rem(col + cores * r, dp)}, device_id_type=MESH)

    def wb_copy(r, c):
        some = pl.ds(c * deep, deep)
        shard = lax.rem(pair + pairs - r, pairs) * cores + core
        return pltpu.make_async_remote_copy(
            src_ref=w_hbm.at[some] if r == 0 else wbuf.at[shard, some], dst_ref=wbuf.at[shard, some],
            send_sem=wb_send.at[r, c], recv_sem=wb_recv.at[r, c],
            device_id={"dp": sibling}, device_id_type=MESH)

    pl.semaphore_wait(barrier, (sp - 1) + (pairs - 1) + (cores - 1))

    for r in range(1, sp):
        ld_copy(r).start()
    for r in range(1, pairs):
        for c in range(cuts):
            wa_copy(r, c).start()

    @pl.loop(0, items)
    def _(i):
        for r in range(1, group):
            for n in range(3):
                x_copy(i, r, n).start()

    if cores == 2:
        for c in range(cuts):
            wb_copy(0, c).start()

    place = lax.broadcasted_iota(jnp.int32, (span, half), 0) + z * span
    order = lax.broadcasted_iota(jnp.int32, (1, half), 1).astype(F32)
    angle = place.astype(F32) * jnp.exp(order * (-math.log(10000.0) / half))
    cos_tab[...] = jnp.cos(angle)
    sin_tab[...] = jnp.sin(angle)

    @pl.when(z == 0)
    def _():
        tin[...] = jnp.zeros_like(tin)

    for copy in local[:4]:
        copy.wait()
    for r in range(1, sp):
        ld_copy(r).wait_recv()
    for n in range(sp):
        ldrows[pl.ds(n * rows, rows), :] = ldbuf[n, :, pl.ds(pl.multiple_of(z * span, span), span)]

    def rotate(field):
        wide = field.astype(F32)
        first, second = wide[:, :half], wide[:, half:]
        cosine, sine = cos_tab[...], sin_tab[...]
        return jnp.concatenate(
            [first * cosine - second * sine, second * cosine + first * sine], axis=1).astype(BF16)

    rank = lax.broadcasted_iota(jnp.int32, (span, span), 0)
    lane = lax.broadcasted_iota(jnp.int32, (span, span), 1)

    def decays(s, hh):
        decay = ldrows[pl.ds(s * heads + x * own + hh, 1), :]
        return decay, jnp.sum(jnp.where(rank >= lane, decay, 0.0), axis=1, keepdims=True)

    def prepare(i):
        s, hh, slot = lax.div(i, own), lax.rem(i, own), lax.rem(i, 2)
        for r in range(1, group):
            for n in range(2):
                x_copy(i, r, n).wait_recv()
        decay, within = decays(s, hh)
        ending = jnp.sum(decay, axis=1, keepdims=True)
        rot_k = rotate(kbuf[s, hh])
        rkbuf[slot] = rot_k
        scaled = (rot_k.astype(F32) * jnp.exp(jnp.minimum(ending - within, 0.0))).astype(BF16)
        fall[slot] = jnp.broadcast_to(jnp.exp(ending), fall.shape[1:])
        ubuf[slot] = lax.dot_general(
            scaled, vbuf[s, hh], (((0,), (0,)), ((), ())), preferred_element_type=F32)

    def advance(i):
        slot = lax.rem(i, 2)
        factor = fall[slot, 0:1, :]
        for p in range(parts):
            @pl.when(z > 0)
            def _():
                t_copy(i, p).wait_recv()

            @pl.when(z < stages - 1)
            def _():
                some = pl.ds(p * slab, slab)
                tout[i, some] = (factor * tin[i, some].astype(F32) + ubuf[slot, some]).astype(BF16)
                t_copy(i, p).start()

    def attend(i):
        s, hh, slot = lax.div(i, own), lax.rem(i, own), lax.rem(i, 2)
        for r in range(1, group):
            x_copy(i, r, 2).wait_recv()
        _, within = decays(s, hh)
        across = jnp.sum(jnp.where(rank == lane, within, 0.0), axis=0, keepdims=True)
        causal = rank >= lane
        mask = jnp.where(causal, jnp.exp(jnp.where(causal, within - across, 0.0)), 0.0)
        rot_q = rotate(qbuf[s, hh])
        scores = lax.dot_general(rot_q, rkbuf[slot], (((1,), (1,)), ((), ())), preferred_element_type=F32)
        weights = (scores * mask).astype(BF16)
        here = jnp.dot(weights, vbuf[s, hh], preferred_element_type=F32)
        carried = jnp.dot(rot_q, tin[i], preferred_element_type=F32)
        retained = (here + jnp.exp(within) * carried).astype(BF16).astype(F32)
        square = jnp.mean(retained * retained, axis=1, keepdims=True)
        obuf[s, hh] = (retained * lax.rsqrt(square + 1e-06)).astype(BF16)
        for r in range(1, group):
            o_copy(i, r).start()
        xbuf[pl.ds(pl.multiple_of(s * seg, seg), seg),
             pl.ds(pl.multiple_of((x * own + hh) * width, width), width)] = obuf[s, hh, mine]

    def pass_w(c):
        for r in range(1, pairs):
            wa_copy(r, c).wait_recv()
            if cores == 2:
                wb_copy(r, c).start()

    def land(first, last):
        @pl.loop(first, last)
        def _(i):
            for r in range(1, group):
                o_copy(i, r).wait_recv()

    def project(first, count):
        land(first * own, (first + count) * own)
        if count:
            some = pl.ds(first * seg, count * seg)

            @pl.loop(0, dp)
            def _(n):
                out_ref[some, pl.ds(pl.multiple_of(n * feats, feats), feats)] = jnp.dot(
                    xbuf[some, :], wbuf[n], preferred_element_type=F32).astype(BF16)

    final = pl.ds((seqs - 1) * seg, seg)

    def heads_of(first, count, n):
        total = jnp.zeros((seg, feats), F32)
        for g in range(group if count else 0):
            some = pl.ds((g * own + first) * width, count * width)
            total = total + jnp.dot(xbuf[final, some], wbuf[n, some, :], preferred_element_type=F32)
        return total

    def most_of_final():
        land((seqs - 1) * own, items - 1)

        @pl.loop(0, dp)
        def _(n):
            most[n] = heads_of(0, own - 1, n)

    def rest_of_final():
        land(items - 1, items)

        @pl.loop(0, dp)
        def _(n):
            out_ref[final, pl.ds(pl.multiple_of(n * feats, feats), feats)] = (
                most[n] + heads_of(own - 1, 1, n)).astype(BF16)

    def whole_w():
        pass_w(cuts - 1)
        local[4].wait()
        if cores == 2:
            for r in range(pairs):
                for c in range(cuts):
                    wb_copy(r, c).wait_recv()

    hold = items * 3 // 4
    prepare(0)

    def turn(i):
        advance(i)
        attend(i)

        @pl.when(i + 1 < items)
        def _():
            prepare(i + 1)

    @pl.loop(0, hold)
    def _(i):
        turn(i)

    for c in range(cuts - 1):
        pass_w(c)

    @pl.loop(hold, items - 2)
    def _(i):
        turn(i)

    early = max(seqs - 2, 0)

    @pl.when(z == stages - 1)
    def _():
        whole_w()
        project(0, early)

    turn(items - 2)

    @pl.when(z == stages - 1)
    def _():
        project(early, seqs - 1 - early)

    turn(items - 1)

    @pl.when(z < stages - 1)
    def _():
        whole_w()
        project(0, seqs - 1)

    most_of_final()
    rest_of_final()

    for r in range(1, sp):
        ld_copy(r).wait_send()
    for c in range(cuts):
        for r in range(1, pairs):
            wa_copy(r, c).wait_send()
        if cores == 2:
            for r in range(pairs):
                wb_copy(r, c).wait_send()

    @pl.loop(0, items)
    def _(i):
        for r in range(1, group):
            for n in range(3):
                x_copy(i, r, n).wait_send()
            o_copy(i, r).wait_send()

        @pl.when(z < stages - 1)
        def _():
            for p in range(parts):
                t_copy(i, p).wait_send()


def on_device(sp, dp, queries, keys, values, log_decay, w_out):
    seqs, heads, seg, width = queries.shape
    rows, length = log_decay.shape
    group = 2 if sp % 2 == 0 and heads % 2 == 0 else 1
    cores = 2 if dp % 2 == 0 else 1
    pairs, own = dp // cores, heads // group
    items, span, half = seqs * own, group * seg, width // 2
    feats = w_out.shape[2]
    parts, cuts = 4, 2
    dma = pltpu.SemaphoreType.DMA
    some = lambda count: max(count, 1)
    hbm = pl.BlockSpec(memory_space=pl.ANY)
    vmem = pl.BlockSpec(memory_space=pltpu.VMEM)
    mixed = pl.pallas_call(
        functools.partial(kernel, (sp, dp, group, cores)),
        out_shape=jax.ShapeDtypeStruct((seqs * seg, dp * feats), BF16),
        in_specs=[hbm, hbm, hbm, hbm, hbm],
        out_specs=vmem,
        scratch_shapes=[
            pltpu.VMEM((seqs, own, span, width), BF16),
            pltpu.VMEM((seqs, own, span, width), BF16),
            pltpu.VMEM((seqs, own, span, width), BF16),
            pltpu.VMEM((sp, rows, length), F32),
            pltpu.VMEM((sp * rows, span), F32),
            pltpu.VMEM((span, half), F32),
            pltpu.VMEM((span, half), F32),
            pltpu.VMEM((dp, heads * width, feats), BF16),
            pltpu.VMEM((items, width, width), BF16),
            pltpu.VMEM((items, width, width), BF16),
            pltpu.VMEM((seqs, own, span, width), BF16),
            pltpu.VMEM((seqs * seg, heads * width), BF16),
            pltpu.VMEM((2, width, width), F32),
            pltpu.VMEM((2, 8, width), F32),
            pltpu.VMEM((2, span, width), BF16),
            pltpu.VMEM((dp, seg, feats), F32),
            dma((5,)),
            dma((some(sp - 1),)), dma((some(sp - 1),)),
            dma((3, some(group - 1), items)), dma((3, some(group - 1), items)),
            dma((items, parts)), dma((items, parts)),
            dma((some(group - 1), items)), dma((some(group - 1), items)),
            dma((some(pairs - 1), cuts)), dma((some(pairs - 1), cuts)),
            dma((pairs, cuts)), dma((pairs, cuts)),
        ],
        compiler_params=pltpu.CompilerParams(
            collective_id=0, has_side_effects=True, vmem_limit_bytes=67043328),
    )(queries, keys, values, log_decay, w_out.reshape(heads * width, feats))
    return mixed.reshape(seqs, seg, dp * feats)


def solution(mesh):
    placed = (
        P("dp", None, "sp", None),
        P("dp", None, "sp", None),
        P("dp", None, "sp", None),
        P(("dp", "sp"), None),
        P(None, None, "dp"),
    )
    body = functools.partial(on_device, mesh.shape["sp"], mesh.shape["dp"])
    return jax.shard_map(
        body, mesh=mesh, in_specs=placed, out_specs=P("dp", "sp", None), check_vma=False
    )
```

time: 77.8 us -> 73.4 us (0.943)
  local copies, waits for them, and re-layouts: 5.34 us -> 2.3 us
  Pallas kernels: 72.2 us -> 71 us
    unnamed x9 -> x1, local copies, waits for them, and re-layouts: 5.34 us -> 2.3 us
    pallas_call x1, Pallas kernels: 72.2 us -> 71 us  [on_device(): pl.pallas_call(functools.partial(kernel, (sp, dp, group, cores)), out_sha...]
where the time goes in v2:
time: 73.4 us; the launch traced here: 73.3 us
  Pallas kernels  71 us (97%)
  local copies, waits for them, and re-layouts  2.3 us (3%)
    pallas_call x1, Pallas kernels, on_device(): pl.pallas_call(functools.partial(kernel, (sp, dp, group, cores)), out_sha...  71 us
    unnamed x1, local copies, waits for them, and re-layouts  2.3 us

profile of v2, /device:TPU:29, one launch (start us, length us, event | category | flops | bytes accessed | tf_op | source)
XLA Modules:
  0.0 73.3 jit_solution(17060903871449226810)
XLA Ops:
  0.0 71.0 %shard_map.55 = bf16[256,2048]{1,0:T(8,128)(2,1)} custom-call(bf16[4,8,64,256]{3,2,1,0:T(8,128)(2,1)} %q_hbm.1, bf16[4,8,64,256]{3,2,1,0:T(8,128)(2,1)} %k_hbm.1, bf16[4,8,64,256]{3,2,1,0:T(8,128)(2,1)} %v_hbm.1, f32[4,512]{1,0:T(4,128)} %ld_hbm.1, bf16[2048,512]{1,0:T(8,128)(2,1)} %bitcast.3), custom_call_target="tpu_custom_call" | custom-call | tf_op jit(solution)/shard_map/pallas_call | solution.py:338
  71.0 2.3 %copy.7 = bf16[4,64,2048]{2,1,0:T(8,128)(2,1)} copy(bf16[4,64,2048]{2,1,0:T(8,128)(2,1)} %bitcast.2) | data formatting | bytes 2097152
